TPU v7x, 32 devices: a whole 2x2x4 slice. The times are simulated.
32 devices in a mesh: kv: 8 (over z, y), tp: 4 (over x, core).
Axes of the slice: x: 2, y: 2, z: 4, core: 2. Of those that a mesh axis runs over, the one named last changes fastest.
Arguments:
- tokens: bfloat16 [32, 4096], P(None, ('kv', 'tp')), may hold values from -36 to 36
- first_gain: float32 [4096], P('kv'), may hold values from 0.1 to 1.9
- first_gate: bfloat16 [4096, 11264], P('kv', 'tp'), may hold values from -0.09375 to 0.09375
- first_up: bfloat16 [4096, 11264], P('kv', 'tp'), may hold values from -0.09375 to 0.09375
- first_down: bfloat16 [11264, 4096], P('tp', 'kv'), may hold values from -0.0546875 to 0.0546875
- mix_gain: float32 [4096], P('kv'), may hold values from 0.1 to 1.9
- w_query: bfloat16 [4096, 2048], P('kv', 'tp'), may hold values from -0.09375 to 0.09375
- key_cache: bfloat16 [32, 8192, 1024], P(None, 'kv', 'tp'), may hold values from -100 to 100
- value_cache: bfloat16 [32, 8192, 1024], P(None, 'kv', 'tp'), may hold values from -6 to 6
- map_weight: float32 [32], P('tp'), may hold values from 0.3 to 0.8
- head_gain: float32 [64], replicated, may hold values from 0.1 to 1.9
- w_out: bfloat16 [2048, 4096], P('tp', 'kv'), may hold values from -0.125 to 0.125
- second_gain: float32 [4096], P('kv'), may hold values from 0.1 to 1.9
- second_gate: bfloat16 [4096, 11264], P('kv', 'tp'), may hold values from -0.09375 to 0.09375
- second_up: bfloat16 [4096, 11264], P('kv', 'tp'), may hold values from -0.09375 to 0.09375
- second_down: bfloat16 [11264, 4096], P('tp', 'kv'), may hold values from -0.0546875 to 0.0546875
Outputs:
- mixed: bfloat16 [32, 4096], P(None, ('kv', 'tp'))
All inputs are finite; a program needn't handle non-finite values.
Results may differ from a plain program's by a relative error of at most 0.0158.
Values may be sent and summed in bfloat16 or wider, within the bound.
A program may use at most 128 MiB of HBM per device.

v0:
```python
import math

import jax
import jax.numpy as jnp
from jax import lax
from jax.sharding import PartitionSpec as P

D = 4096
HEAD = 64


EPS = 1e-06
HEAD_SCALE = 0.8


def merged(value, axis, join):
    pieces = jax.tree.map(lambda part: lax.all_gather(part, axis), value)
    head = jax.tree.map(lambda part: part[0], pieces)
    tail = jax.tree.map(lambda part: part[1:], pieces)
    subtotal, _ = lax.scan(lambda subtotal, piece: (join(subtotal, piece), None), head, tail)
    return subtotal


def norm_total(squares):
    return lax.psum(squares, "kv")


def channel_mixer(residual, gain, w_gate, w_up, w_down):
    squares = jnp.sum(residual * residual, axis=1, keepdims=True)
    scaled = (residual * gain).astype(jnp.bfloat16)
    part_gate = jnp.dot(scaled, w_gate, preferred_element_type=jnp.float32)
    part_up = jnp.dot(scaled, w_up, preferred_element_type=jnp.float32)
    row_total = norm_total(squares)
    gate_sum, up_sum = lax.psum((part_gate, part_up), "kv")
    factor = lax.rsqrt(row_total / D + EPS)
    active = (jax.nn.silu(gate_sum * factor) * (up_sum * factor)).astype(jnp.bfloat16)
    partial_value = jnp.dot(active, w_down, preferred_element_type=jnp.float32)
    return lax.psum(partial_value, "tp")


def merge_pair(first, second):
    row_peak = jnp.maximum(first[0], second[0])
    scale_first = jnp.exp(first[0] - row_peak)
    scale_second = jnp.exp(second[0] - row_peak)
    return (
        row_peak,
        first[1] * scale_first + second[1] * scale_second,
        first[2] * scale_first[..., None] + second[2] * scale_second[..., None],
    )


def combine_maps(earlier, later):
    return merge_pair(earlier[:3], later[:3]) + merge_pair(earlier[3:], later[3:])


def attention_mix(
    residual, mix_gain, w_query, key_cache, value_cache, map_weight, head_gain, w_out
):
    squares = jnp.sum(residual * residual, axis=1, keepdims=True)
    scaled = (residual * mix_gain).astype(jnp.bfloat16)
    part_query = jnp.dot(scaled, w_query, preferred_element_type=jnp.float32)
    row_total = norm_total(squares)
    queries = lax.psum(part_query, "kv")
    queries = (queries * lax.rsqrt(row_total / D + EPS)).astype(jnp.bfloat16)
    batch_rows = queries.shape[0]
    kv_local = key_cache.shape[2] // HEAD
    group = queries.shape[1] // (kv_local * HEAD)
    queries = queries.reshape(batch_rows, kv_local, group, HEAD)
    cached = key_cache.reshape(batch_rows, -1, kv_local, HEAD)
    stored = value_cache.reshape(batch_rows, -1, kv_local, HEAD)

    def partial_map(first_col, last_col):
        scores = jnp.einsum(
            "bkgd,bpkd->bkgp",
            queries[..., first_col:last_col],
            cached[..., first_col:last_col],
            preferred_element_type=jnp.float32,
        ) / math.sqrt(last_col - first_col)
        row_peak = jnp.max(scores, axis=3)
        exp_terms = jnp.exp(scores - row_peak[..., None])
        weights_sum = jnp.sum(exp_terms, axis=3)
        summed = jnp.einsum(
            "bkgp,bpkd->bkgd",
            exp_terms.astype(jnp.bfloat16),
            stored,
            preferred_element_type=jnp.float32,
        )
        return (row_peak, weights_sum, summed)

    half_dim = HEAD // 2
    peak_one, sum_one, out_one = partial_map(0, half_dim)
    peak_two, sum_two, out_two = partial_map(half_dim, HEAD)
    peak_one, sum_one, out_one, peak_two, sum_two, out_two = merged(
        (peak_one, sum_one, out_one, peak_two, sum_two, out_two), "kv", combine_maps
    )
    weight = map_weight.reshape(kv_local, group)
    combined = out_one / sum_one[..., None] - weight[..., None] * out_two / sum_two[..., None]
    normed = (
        combined
        * lax.rsqrt(jnp.mean(combined * combined, axis=3, keepdims=True) + EPS)
        * head_gain
        * HEAD_SCALE
    )
    normed = normed.astype(jnp.bfloat16).reshape(batch_rows, kv_local * group * HEAD)
    partial_value = jnp.dot(normed, w_out, preferred_element_type=jnp.float32)
    return lax.psum(partial_value, "tp")


def on_device(
    tokens,
    first_gain,
    first_gate,
    first_up,
    first_down,
    mix_gain,
    w_query,
    key_cache,
    value_cache,
    map_weight,
    head_gain,
    w_out,
    second_gain,
    second_gate,
    second_up,
    second_down,
):
    residual = lax.all_gather(tokens, "tp", axis=1, tiled=True).astype(jnp.float32)
    residual = residual + 0.5 * channel_mixer(
        residual, first_gain, first_gate, first_up, first_down
    )
    residual = residual + attention_mix(
        residual, mix_gain, w_query, key_cache, value_cache, map_weight, head_gain, w_out
    )
    residual = residual + 0.5 * channel_mixer(
        residual, second_gain, second_gate, second_up, second_down
    )
    width = residual.shape[1] // lax.axis_size("tp")
    return lax.dynamic_slice_in_dim(residual, lax.axis_index("tp") * width, width, 1).astype(
        jnp.bfloat16
    )


def solution(mesh):
    placed = (
        P(None, ("kv", "tp")),
        P("kv"),
        P("kv", "tp"),
        P("kv", "tp"),
        P("tp", "kv"),
        P("kv"),
        P("kv", "tp"),
        P(None, "kv", "tp"),
        P(None, "kv", "tp"),
        P("tp"),
        P(),
        P("tp", "kv"),
        P("kv"),
        P("kv", "tp"),
        P("kv", "tp"),
        P("tp", "kv"),
    )
    return jax.shard_map(
        on_device, mesh=mesh, in_specs=placed, out_specs=P(None, ("kv", "tp")), check_vma=False
    )
```

profile of v0, /device:TPU:0, one launch (start us, length us, event | category | flops | bytes accessed | tf_op | source)
XLA Modules:
  0.0 626.8 jit_solution(4104942960489870407)
XLA Ops:
  6.5 6.5 %all_gather.39 = bf16[32,512]{1,0:T(8,128)(2,1)S(1)} all-gather(bf16[32,128]{1,0:T(8,128)(2,1)} %param.18), channel_id=1, replica_groups=mesh['kv'=8,'tp'=4] {'tp'}, dimensions={1}, use_global_device_ids=true | all-gather | bytes 40960 | tf_op jit(solution)/shard_map/all_gather | solution.py:127
  16.6 22.7 %psum.78 = f32[32,1]{0,1:T(1,128)S(1)} all-reduce(f32[32,1]{0,1:T(1,128)S(1)} %bitcast.79), channel_id=1, replica_groups=mesh['kv'=8,'tp'=4] {'kv'}, use_global_device_ids=true, to_apply=%region_2.0 | all-reduce | flops 32 | bytes 256 | tf_op jit(solution)/shard_map/psum | solution.py:25
  39.3 53.8 %all-reduce.19.cloned.1.call-done = (f32[32,2816]{1,0:T(8,128)}, f32[32,2816]{1,0:T(8,128)}) async-done(((f32[32,2816]{1,0:T(8,128)}, f32[32,2816]{1,0:T(8,128)}), (f32[32,2816]{1,0:T(8,128)}, f32[32,2816]{1,0:T(8,128)})) %all-reduce.19.cloned.1.call-update) | async-done | bytes 720912 | tf_op jit(solution)/shard_map/psum | solution.py:34
  95.6 22.5 %copy.107 = bf16[32,1024,256]{1,2,0:T(8,128)(2,1)} copy(bf16[32,1024,256]{2,1,0:T(8,128)(2,1)} %param.25) | data formatting | bytes 33554432 | tf_op args[7]
  118.2 22.6 %copy.110 = bf16[32,1024,256]{1,2,0:T(8,128)(2,1)} copy(bf16[32,1024,256]{2,1,0:T(8,128)(2,1)} %param.26) | data formatting | bytes 33554432 | tf_op args[8]
  141.7 19.6 %psum.82 = f32[32,1]{0,1:T(1,128)S(1)} all-reduce(f32[32,1]{0,1:T(1,128)S(1)} %bitcast.80), channel_id=1, replica_groups=mesh['kv'=8,'tp'=4] {'kv'}, use_global_device_ids=true, to_apply=%region_7.8 | all-reduce | flops 32 | bytes 256 | tf_op jit(solution)/shard_map/psum | solution.py:25
  163.1 66.6 %all-reduce.11.cloned.1.call-done = f32[32,512]{1,0:T(8,128)} async-done(((f32[32,512]{1,0:T(8,128)}), f32[32,512]{1,0:T(8,128)}) %all-reduce.11.cloned.1.call-update) | async-done | bytes 65552 | tf_op jit(solution)/shard_map/psum | solution.py:63
  230.7 4.9 fusion.55
  235.6 4.9 fusion.54
  242.0 30.9 %all-gather.1 = f32[256,4,2]{1,2,0:T(2,128)S(1)} all-gather(f32[32,4,2]{1,2,0:T(2,128)S(1)} %copy.109), channel_id=3, replica_groups=mesh['kv'=8,'tp'=4] {'kv'}, dimensions={0}, use_global_device_ids=true | all-gather | bytes 9216 | tf_op jit(solution)/shard_map/all_gather | solution.py:17
  274.5 30.9 %all-gather.4 = f32[256,4,2]{1,2,0:T(2,128)S(1)} all-gather(f32[32,4,2]{1,2,0:T(2,128)S(1)} %copy.113), channel_id=6, replica_groups=mesh['kv'=8,'tp'=4] {'kv'}, dimensions={0}, use_global_device_ids=true | all-gather | bytes 9216 | tf_op jit(solution)/shard_map/all_gather | solution.py:17
  305.4 31.0 %all-gather = f32[256,4,2]{1,2,0:T(2,128)S(1)} all-gather(f32[32,4,2]{1,2,0:T(2,128)S(1)} %copy.108), channel_id=2, replica_groups=mesh['kv'=8,'tp'=4] {'kv'}, dimensions={0}, use_global_device_ids=true | all-gather | bytes 9216 | tf_op jit(solution)/shard_map/all_gather | solution.py:17
  337.1 31.1 %all-gather.3 = f32[256,4,2]{1,2,0:T(2,128)S(1)} all-gather(f32[32,4,2]{1,2,0:T(2,128)S(1)} %copy.112), channel_id=5, replica_groups=mesh['kv'=8,'tp'=4] {'kv'}, dimensions={0}, use_global_device_ids=true | all-gather | bytes 9216 | tf_op jit(solution)/shard_map/all_gather | solution.py:17
  369.0 8.8 %fusion.22 = f32[32,4,2,64]{3,2,1,0:T(2,128)} fusion(bf16[32,1024,4,64]{1,3,2,0:T(8,128)(2,1)} %bitcast.68, f32[32,4,2,1024]{3,2,1,0:T(2,128)S(1)} %get-tuple-element.178, f32[32,4,2]{2,1,0:T(4,128)S(1)} %get-tuple-element.177), kind=kOutput, calls=%fused_computation.32 | convolution fusion | flops 34078720 | bytes 17892352 | tf_op jit(solution)/shard_map/bkgp,bpkd->bkgd/dot_general | solution.py:82
  377.8 8.2 %fusion.24 = f32[32,4,2,64]{3,2,1,0:T(2,128)S(1)} fusion(bf16[32,1024,4,64]{1,3,2,0:T(8,128)(2,1)} %bitcast.69, f32[32,4,2,1024]{3,2,1,0:T(2,128)S(1)} %get-tuple-element.176, f32[32,4,2]{2,1,0:T(4,128)S(1)} %get-tuple-element.175), kind=kOutput, calls=%fused_computation.33 | convolution fusion | flops 34078720 | bytes 17892352 | tf_op jit(solution)/shard_map/bkgp,bpkd->bkgd/dot_general | solution.py:82
  386.0 32.9 %all-gather.5 = f32[256,4,2,64]{3,1,2,0:T(4,128)S(1)} all-gather(f32[32,4,2,64]{3,1,2,0:T(4,128)S(1)} %copy.114), channel_id=7, replica_groups=mesh['kv'=8,'tp'=4] {'kv'}, dimensions={0}, use_global_device_ids=true | all-gather | bytes 589824 | tf_op jit(solution)/shard_map/all_gather | solution.py:17
  419.8 32.1 %all-gather.2 = f32[256,4,2,64]{3,1,2,0:T(4,128)S(1)} all-gather(f32[32,4,2,64]{3,1,2,0:T(4,128)S(1)} %copy.111), channel_id=4, replica_groups=mesh['kv'=8,'tp'=4] {'kv'}, dimensions={0}, use_global_device_ids=true | all-gather | bytes 589824 | tf_op jit(solution)/shard_map/all_gather | solution.py:17
  457.6 11.1 %while.20 = (s32[]{:T(128)}, f32[32,4,2]{0,2,1:T(2,128)S(1)}, f32[32,4,2]{0,2,1:T(2,128)S(1)}, f32[32,4,2,64]{3,2,1,0:T(2,128)S(1)}, f32[32,4,2]{0,2,1:T(2,128)S...) while((s32[]{:T(128)}, f32[32,4,2]{0,2,1:T(2,128)S(1)}, ...), condition=%wide.region_13.14_spmd, body=%wide.region_12.13_spmd.sunk | while | flops 101378 | bytes 684189 | solution.py:20
  470.9 31.2 %all-reduce.13.cloned.1.call-done = f32[32,512]{1,0:T(8,128)} async-done(((f32[32,512]{1,0:T(8,128)}), f32[32,512]{1,0:T(8,128)}) %all-reduce.13.cloned.1.call-update) | async-done | bytes 65552 | tf_op jit(solution)/shard_map/psum | solution.py:106
  506.2 3.3 fusion.47
  509.6 21.5 %psum.85 = f32[32,1]{0,1:T(1,128)S(1)} all-reduce(f32[32,1]{0,1:T(1,128)S(1)} %bitcast.78), channel_id=1, replica_groups=mesh['kv'=8,'tp'=4] {'kv'}, use_global_device_ids=true, to_apply=%region_18.19 | all-reduce | flops 32 | bytes 256 | tf_op jit(solution)/shard_map/psum | solution.py:25
  531.1 53.4 %all-reduce.17.cloned.1.call-done = (f32[32,2816]{1,0:T(8,128)}, f32[32,2816]{1,0:T(8,128)}) async-done(((f32[32,2816]{1,0:T(8,128)}, f32[32,2816]{1,0:T(8,128)}), (f32[32,2816]{1,0:T(8,128)}, f32[32,2816]{1,0:T(8,128)})) %all-reduce.17.cloned.1.call-update) | async-done | bytes 720912 | tf_op jit(solution)/shard_map/psum | solution.py:34
  584.5 3.3 fusion.29
  587.8 30.8 %all-reduce.15.cloned.1.call-done = f32[32,512]{1,0:T(8,128)} async-done(((f32[32,512]{1,0:T(8,128)}), f32[32,512]{1,0:T(8,128)}) %all-reduce.15.cloned.1.call-update) | async-done | bytes 65552 | tf_op jit(solution)/shard_map/psum | solution.py:38
  (170 shorter events, 39.4 us)
Async XLA Ops:
  6.5 86.6 %all-reduce.19.cloned.1.call-start = ((), (), s32[]{:S(2)}) async-start(), calls=%async_computation.5 | async-start | bytes 1441792 | tf_op jit(solution)/shard_map/psum | solution.py:34
  15.0 78.1 %copy-start.3 = (bf16[2816,512]{1,0:T(8,128)(2,1)S(1)}, bf16[2816,512]{1,0:T(8,128)(2,1)}, u32[]{:S(2)}) copy-start(bf16[2816,512]{1,0:T(8,128)(2,1)} %param.22) | copy-start | bytes 8650756
  16.4 79.2 %copy-start.16 = (f32[8]{0:T(128)S(1)}, f32[8]{0:T(128)}, u32[]{:S(2)}) copy-start(f32[8]{0:T(128)} %param.27) | copy-start | bytes 100
  16.4 124.3 %all-reduce.9.cloned.1.call-start = ((), (), s32[]{:S(2)}) async-start(), calls=%async_computation | async-start | bytes 131072 | tf_op jit(solution)/shard_map/psum | solution.py:38
  95.5 134.1 %all-reduce.11.cloned.1.call-start = ((), (), s32[]{:S(2)}) async-start(), calls=%async_computation.1 | async-start | bytes 131072 | tf_op jit(solution)/shard_map/psum | solution.py:63
  118.2 43.1 %copy-start.10 = (bf16[512,512]{1,0:T(8,128)(2,1)S(1)}, bf16[512,512]{1,0:T(8,128)(2,1)}, u32[]{:S(2)}) copy-start(bf16[512,512]{1,0:T(8,128)(2,1)} %param.24) | copy-start | bytes 1572868
  118.2 43.1 %copy-start.14 = (f32[512]{0:T(512)S(1)}, f32[512]{0:T(512)}, u32[]{:S(2)}) copy-start(f32[512]{0:T(512)} %param.23) | copy-start | bytes 6148
  163.0 339.1 %all-reduce.13.cloned.1.call-start = ((), (), s32[]{:S(2)}) async-start(), calls=%async_computation.2 | async-start | bytes 131072 | tf_op jit(solution)/shard_map/psum | solution.py:106
  272.9 104.9 %copy-start.4 = (f32[256,4,2]{1,2,0:T(2,128)}, f32[256,4,2]{1,2,0:T(2,128)S(1)}, u32[]{:S(2)}) copy-start(f32[256,4,2]{1,2,0:T(2,128)S(1)} %all-gather.1) | copy-start | bytes 24580
  305.4 72.4 %copy-start.5 = (f32[256,4,2]{1,2,0:T(2,128)}, f32[256,4,2]{1,2,0:T(2,128)S(1)}, u32[]{:S(2)}) copy-start(f32[256,4,2]{1,2,0:T(2,128)S(1)} %all-gather.4) | copy-start | bytes 24580
  336.4 41.4 %copy-start.6 = (f32[256,4,2]{1,2,0:T(2,128)}, f32[256,4,2]{1,2,0:T(2,128)S(1)}, u32[]{:S(2)}) copy-start(f32[256,4,2]{1,2,0:T(2,128)S(1)} %all-gather) | copy-start | bytes 24580
  418.9 33.8 %slice-start = ((f32[256,4,2]{1,2,0:T(2,128)}), f32[32,4,2]{1,2,0:T(2,128)S(1)}, s32[]{:S(2)}) async-start(f32[256,4,2]{1,2,0:T(2,128)} %copy-done.4), calls=%async_computation.6 | async-start | bytes 65536 | tf_op jit(solution)/shard_map/slice | solution.py:18
  418.9 33.9 %slice-start.1 = ((f32[256,4,2]{1,2,0:T(2,128)}), f32[224,4,2]{1,2,0:T(2,128)S(1)}, s32[]{:S(2)}) async-start(f32[256,4,2]{1,2,0:T(2,128)} %copy-done.4), calls=%async_computation.7 | async-start | bytes 458752 | tf_op jit(solution)/shard_map/slice | solution.py:19
  419.5 33.4 %slice-start.2 = ((f32[256,4,2]{1,2,0:T(2,128)}), f32[32,4,2]{1,2,0:T(2,128)S(1)}, s32[]{:S(2)}) async-start(f32[256,4,2]{1,2,0:T(2,128)} %copy-done.5), calls=%async_computation.8 | async-start | bytes 65536 | tf_op jit(solution)/shard_map/slice | solution.py:18
  419.6 33.5 %slice-start.3 = ((f32[256,4,2]{1,2,0:T(2,128)}), f32[224,4,2]{1,2,0:T(2,128)S(1)}, s32[]{:S(2)}) async-start(f32[256,4,2]{1,2,0:T(2,128)} %copy-done.5), calls=%async_computation.9 | async-start | bytes 458752 | tf_op jit(solution)/shard_map/slice | solution.py:19
  419.6 33.6 %slice-start.4 = ((f32[256,4,2]{1,2,0:T(2,128)}), f32[32,4,2]{1,2,0:T(2,128)S(1)}, s32[]{:S(2)}) async-start(f32[256,4,2]{1,2,0:T(2,128)} %copy-done.6), calls=%async_computation.10 | async-start | bytes 65536 | tf_op jit(solution)/shard_map/slice | solution.py:18
  419.6 34.8 %slice-start.5 = ((f32[256,4,2]{1,2,0:T(2,128)}), f32[32,4,2]{1,2,0:T(2,128)S(1)}, s32[]{:S(2)}) async-start(f32[256,4,2]{1,2,0:T(2,128)} %copy-done.7), calls=%async_computation.11 | async-start | bytes 65536 | tf_op jit(solution)/shard_map/slice | solution.py:18
  457.5 12.1 %copy-start.15 = (f32[64]{0:T(128)S(1)}, f32[64]{0:T(128)}, u32[]{:S(2)}) copy-start(f32[64]{0:T(128)} %param.28) | copy-start | bytes 772
  457.5 12.5 %copy-start.9 = (bf16[512,512]{1,0:T(8,128)(2,1)S(1)}, bf16[512,512]{1,0:T(8,128)(2,1)}, u32[]{:S(2)}) copy-start(bf16[512,512]{1,0:T(8,128)(2,1)} %param.29) | copy-start | bytes 1572868
  457.5 44.6 %copy-start.8 = (f32[32,512]{1,0:T(8,128)S(1)}, f32[32,512]{1,0:T(8,128)}, u32[]{:S(2)}) copy-start(f32[32,512]{1,0:T(8,128)} %all-reduce.9.cloned.1.call-done) | copy-start | bytes 196612
  457.6 45.5 %copy-start.13 = (f32[512]{0:T(512)S(1)}, f32[512]{0:T(512)}, u32[]{:S(2)}) copy-start(f32[512]{0:T(512)} %param.30) | copy-start | bytes 6148
  470.9 113.6 %all-reduce.17.cloned.1.call-start = ((), (), s32[]{:S(2)}) async-start(), calls=%async_computation.4 | async-start | bytes 1441792 | tf_op jit(solution)/shard_map/psum | solution.py:34
  506.2 113.8 %copy-start.1 = (bf16[512,2816]{1,0:T(8,128)(2,1)S(1)}, bf16[512,2816]{1,0:T(8,128)(2,1)}, u32[]{:S(2)}) copy-start(bf16[512,2816]{1,0:T(8,128)(2,1)} %param.21) | copy-start | bytes 8650756
  509.6 109.1 %all-reduce.15.cloned.1.call-start = ((), (), s32[]{:S(2)}) async-start(), calls=%async_computation.3 | async-start | bytes 131072 | tf_op jit(solution)/shard_map/psum | solution.py:38
  (5 other events, 41.2 us)
Sparse Core Ops, SparseCore 0:
  16.5 76.5 all-reduce.18
  95.6 30.6 all-reduce.8
  163.1 66.4 all-reduce.10
  471.0 31.0 all-reduce.12
  509.7 74.7 all-reduce.16
  588.0 30.6 all-reduce.14
where the time goes:
time: 629 us; the launch traced here: 627 us
  blocking collectives  259 us (41%)
  waiting for transfers between devices  236 us (38%)
  local copies, waits for them, and re-layouts  58.6 us (9%)
  matrix products  44.7 us (7%)
  other arithmetic  14.3 us (2%)
  between operations  13.7 us (2%)
    all_gather x6, blocking collectives, merged(): pieces = jax.tree.map(lambda part: lax.all_gather(part, axis), value)  189 us
    psum x2, waiting for transfers between devices, channel_mixer(): gate_sum, up_sum = lax.psum((part_gate, part_up), 'kv')  107 us
    psum x1, waiting for transfers between devices, attention_mix(): queries = lax.psum(part_query, 'kv')  66.6 us
    psum x3, blocking collectives, norm_total(): return lax.psum(squares, 'kv')  63.8 us
    unnamed x36, local copies, waits for them, and re-layouts  45.2 us
    psum x1, waiting for transfers between devices, attention_mix(): return lax.psum(partial_value, 'tp')  31.2 us
    psum x2, waiting for transfers between devices, channel_mixer(): return lax.psum(partial_value, 'tp')  30.8 us
    dot_general x2, matrix products, partial_map(): jnp.einsum('bkgp,bpkd->bkgd', exp_terms.astype(jnp.bfloat16), stored, pre...  16.9 us
  transfers between devices with their start and end apart: 6, of which 5 were waited for; matrix products, arithmetic and copies ran while one was open for 7% of the time, Pallas kernels for 0%

commit v1 on v0

v1 whole, which is shorter than its diff:
```python
import functools
import math

import jax
import jax.numpy as jnp
from jax import lax
from jax.experimental import pallas as pl
from jax.experimental.pallas import tpu as pltpu
from jax.sharding import PartitionSpec as P

HEAD = 64
MAPS = 2
LANES = 128
TILE = 8
EPS = 1e-06
HEAD_SCALE = 0.8
F32 = jnp.float32
BF16 = jnp.bfloat16
MESH = pl.DeviceIdType.MESH
VMEM_LIMIT = 60 * 1024 * 1024


def greet(axes):
    barrier = pltpu.get_barrier_semaphore()
    total = 0
    for axis, n in axes:
        me = lax.axis_index(axis)
        for k in range(1, n):
            pl.semaphore_signal(
                barrier, inc=1, device_id={axis: lax.rem(me + k, n)}, device_id_type=MESH
            )
        total += n - 1
    pl.semaphore_wait(barrier, total)


def exchange(axis, n, source, target, sems):
    me = lax.axis_index(axis)
    copies = []
    for k in range(1, n):
        dest = lax.rem(me + k, n)
        copy = pltpu.make_async_remote_copy(
            src_ref=source(dest),
            dst_ref=target(k - 1),
            send_sem=sems.at[0, k - 1],
            recv_sem=sems.at[1, k - 1],
            device_id={axis: dest},
            device_id_type=MESH,
        )
        copy.start()
        copies.append(copy)
    return copies


def total_of(copies, own, recv):
    total = own
    for k, copy in enumerate(copies):
        copy.wait()
        total = total + recv[k].astype(F32)
    return total


def squares_tile(h):
    s = jnp.sum(h * h, axis=1, keepdims=True)
    high = s.astype(BF16).astype(F32)
    lane = lax.broadcasted_iota(jnp.int32, (h.shape[0], LANES), 1)
    return jnp.where(lane < LANES // 2, high, s - high).astype(BF16)


def row_factor(tile, width):
    s = tile[:, :1] + tile[:, LANES // 2 : LANES // 2 + 1]
    return lax.rsqrt(s / width + EPS)


def chunk_width(hidden, n):
    return -(-hidden // (LANES * n)) * LANES


def dot(a, b):
    return jnp.dot(a, b, preferred_element_type=F32)


def feed_forward(n_kv, h, gain, w_gate, w_up, w_down, loads, scratch):
    send, recv, act_own, act_all, rs_sems, ag_sems = scratch
    me = lax.axis_index("kv")
    hidden = w_gate.shape[1]
    cw = chunk_width(hidden, n_kv)
    rows = h.shape[0]
    tile = squares_tile(h)
    scaled = (h * gain).astype(BF16)
    loads[0].wait()
    loads[1].wait()
    for j in range(n_kv):
        low = min(j * cw, hidden)
        w = min(cw, hidden - low)
        for base, weight in ((0, w_gate), (cw, w_up)):
            if w > 0:
                send[j, :, base : base + w] = dot(scaled, weight[:, low : low + w]).astype(BF16)
            if w < cw:
                send[j, :, base + w : base + cw] = jnp.zeros((rows, cw - w), BF16)
        send[j, :, 2 * cw :] = tile
    copies = exchange("kv", n_kv, lambda d: send.at[d], lambda k: recv.at[k], rs_sems)
    total = total_of(copies, send[me].astype(F32), recv)
    factor = row_factor(total[:, 2 * cw :], h.shape[1] * n_kv)
    gate = total[:, :cw] * factor
    up = total[:, cw : 2 * cw] * factor
    act = (gate / (1.0 + jnp.exp(-gate)) * up).astype(BF16)
    act_own[...] = act
    mine = pl.ds(pl.multiple_of(me * cw, LANES), cw)
    act_all[:, mine] = act
    copies = exchange("kv", n_kv, lambda d: act_own, lambda k: act_all.at[:, mine], ag_sems)
    for copy in copies:
        copy.wait()
    loads[2].wait()
    return dot(act_all[:, :hidden], w_down[...])


def sum_over_tp(n_tp, part, send, recv, sems):
    send[...] = part.astype(BF16)
    copies = exchange("tp", n_tp, lambda d: send, lambda k: recv.at[k], sems)
    return total_of(copies, send[...].astype(F32), recv)


def start_loads(pairs, sems):
    loads = [pltpu.make_async_copy(a, b, sems.at[i]) for i, (a, b) in enumerate(pairs)]
    for load in loads:
        load.start()
    return loads


def first_kernel(
    n_kv, n_tp, tokens, gain, mix_gain, gate_any, up_any, down_any, query_any, h_out, q_out,
    w_gate, w_up, w_down, w_query, tok_all, rs_send, rs_recv, act_own, act_all,
    tp_send, tp_recv, q_send, q_recv, load_sems, tok_sems, rs_sems, ag_sems, tp_sems, q_sems,
):
    loads = start_loads(
        ((gate_any, w_gate), (up_any, w_up), (down_any, w_down), (query_any, w_query)), load_sems
    )
    greet((("kv", n_kv), ("tp", n_tp)))
    tp = lax.axis_index("tp")
    tok_all[tp] = tokens[...]
    copies = exchange("tp", n_tp, lambda d: tokens, lambda k: tok_all.at[tp], tok_sems)
    for copy in copies:
        copy.wait()
    h = jnp.concatenate([tok_all[j].astype(F32) for j in range(n_tp)], axis=1)
    part = feed_forward(
        n_kv, h, gain[...], w_gate, w_up, w_down, loads,
        (rs_send, rs_recv, act_own, act_all, rs_sems, ag_sems),
    )
    h = h + 0.5 * sum_over_tp(n_tp, part, tp_send, tp_recv, tp_sems)
    h_out[...] = h
    loads[3].wait()
    columns = w_query.shape[1]
    q_send[:, :columns] = dot((h * mix_gain[...]).astype(BF16), w_query[...]).astype(BF16)
    q_send[:, columns:] = squares_tile(h)
    copies = exchange("kv", n_kv, lambda d: q_send, lambda k: q_recv.at[k], q_sems)
    total = total_of(copies, q_send[...].astype(F32), q_recv)
    factor = row_factor(total[:, columns:], h.shape[1] * n_kv)
    q_out[...] = (total[:, :columns] * factor).astype(BF16)


def attention_kernel(kv_local, per_tile, scale, q_ref, k_ref, v_ref, o_ref, lse_ref):
    wide = lax.broadcasted_iota(jnp.int32, (TILE, kv_local * HEAD), 1) // HEAD
    lane = lax.broadcasted_iota(jnp.int32, (TILE, LANES), 1)
    part_rows = TILE // per_tile
    wide_row = lax.broadcasted_iota(jnp.int32, (TILE, kv_local * HEAD), 0) // part_rows
    lane_row = lax.broadcasted_iota(jnp.int32, (TILE, LANES), 0) // part_rows
    tiles_o, tiles_lse = [], []
    for first in range(0, q_ref.shape[0], per_tile):
        tile_o = jnp.zeros((TILE, kv_local * HEAD), F32)
        tile_lse = jnp.zeros((TILE, LANES), F32)
        for i in range(per_tile):
            b = first + i
            s = scale * lax.dot_general(
                q_ref[b], k_ref[b], (((1,), (1,)), ((), ())), preferred_element_type=F32
            )
            peak = jnp.max(s, axis=1, keepdims=True)
            e = jnp.exp(s - peak)
            l = jnp.sum(e, axis=1, keepdims=True)
            o = dot(e.astype(BF16), v_ref[b]) / l
            lse = peak + jnp.log(l)
            for k in range(kv_local):
                rows = slice(k * TILE, (k + 1) * TILE)
                tile_o = jnp.where((wide == k) & (wide_row == i), o[rows], tile_o)
                tile_lse = jnp.where((lane == k) & (lane_row == i), lse[rows], tile_lse)
        tiles_o.append(tile_o)
        tiles_lse.append(tile_lse)
    o_ref[0] = jnp.concatenate(tiles_o, axis=0).astype(BF16)
    lse_ref[0] = jnp.concatenate(tiles_lse, axis=0)


def second_kernel(
    n_kv, n_tp, kv_local, group, h_in, o_part, lse_part, map_weight, head_gain, gain,
    out_any, gate_any, up_any, down_any, mixed,
    w_out, w_gate, w_up, w_down, o_recv, lse_recv, head_own, head_all, rs_send, rs_recv,
    act_own, act_all, tp_send, tp_recv, fin_send, fin_recv,
    load_sems, o_sems, lse_sems, head_sems, rs_sems, ag_sems, tp_sems, fin_sems,
):
    loads = start_loads(
        ((out_any, w_out), (gate_any, w_gate), (up_any, w_up), (down_any, w_down)), load_sems
    )
    greet((("kv", n_kv), ("tp", n_tp)))
    me = lax.axis_index("kv")
    copies = exchange("kv", n_kv, lambda d: o_part.at[d], lambda k: o_recv.at[k], o_sems)
    copies += exchange("kv", n_kv, lambda d: lse_part.at[d], lambda k: lse_recv.at[k], lse_sems)
    for copy in copies:
        copy.wait()
    lses = [lse_part[me]] + [lse_recv[k] for k in range(n_kv - 1)]
    outs = [o_part[me].astype(F32)] + [o_recv[k].astype(F32) for k in range(n_kv - 1)]
    peak = functools.reduce(jnp.maximum, lses)
    weights = [jnp.exp(lse - peak) for lse in lses]
    scale = 1.0 / functools.reduce(jnp.add, weights)
    slab = outs[0].shape
    head_of = lax.broadcasted_iota(jnp.int32, slab, 1) // HEAD

    def widen(value):
        wide = jnp.zeros(slab, F32)
        for k in range(kv_local):
            wide = jnp.where(head_of == k, value[:, k : k + 1], wide)
        return wide

    merged = functools.reduce(
        jnp.add, [widen(weight * scale) * out for weight, out in zip(weights, outs)]
    )
    diff = merged - map_weight[...] * pltpu.roll(merged, slab[0] - group, 0)
    square = diff * diff
    mean = jnp.zeros(slab, F32)
    for k in range(kv_local):
        here = jnp.sum(jnp.where(head_of == k, square, 0.0), axis=1, keepdims=True) / HEAD
        mean = jnp.where(head_of == k, here, mean)
    head_own[...] = (diff * lax.rsqrt(mean + EPS) * head_gain[...] * HEAD_SCALE).astype(BF16)
    head_all[me] = head_own[...]
    copies = exchange("kv", n_kv, lambda d: head_own, lambda k: head_all.at[me], head_sems)
    for copy in copies:
        copy.wait()
    heads = head_all[...].reshape(n_kv * slab[0], slab[1])
    loads[0].wait()
    batch = h_in.shape[0]
    pick_row = lax.broadcasted_iota(jnp.int32, (batch, heads.shape[0]), 0)
    pick_col = lax.broadcasted_iota(jnp.int32, (batch, heads.shape[0]), 1)
    part = None
    for g in range(group):
        pick = jnp.where(pick_col == pick_row * (MAPS * group) + g, 1.0, 0.0).astype(BF16)
        picked = dot(pick, heads).astype(BF16)
        weight = jnp.concatenate(
            [w_out[(k * group + g) * HEAD : (k * group + g + 1) * HEAD, :] for k in range(kv_local)],
            axis=0,
        )
        term = dot(picked, weight)
        part = term if part is None else part + term
    h = h_in[...] + sum_over_tp(n_tp, part, tp_send, tp_recv, tp_sems)
    part = feed_forward(
        n_kv, h, gain[...], w_gate, w_up, w_down, loads[1:],
        (rs_send, rs_recv, act_own, act_all, rs_sems, ag_sems),
    )
    width = mixed.shape[1]
    tp = lax.axis_index("tp")
    mine = jnp.zeros((batch, width), F32)
    for j in range(n_tp):
        columns = slice(j * width, (j + 1) * width)
        fin_send[j] = part[:, columns].astype(BF16)
        mine = jnp.where(tp == j, h[:, columns], mine)
    copies = exchange("tp", n_tp, lambda d: fin_send.at[d], lambda k: fin_recv.at[k], fin_sems)
    total = total_of(copies, fin_send[tp].astype(F32), fin_recv)
    mixed[...] = (mine + 0.5 * total).astype(BF16)


def dma_sems(n):
    return pltpu.SemaphoreType.DMA((2, n - 1))


def on_device(
    n_kv, n_tp, tokens, first_gain, first_gate, first_up, first_down, mix_gain, w_query,
    key_cache, value_cache, map_weight, head_gain, w_out, second_gain, second_gate, second_up,
    second_down,
):
    batch = tokens.shape[0]
    depth, hidden = first_gate.shape
    length = key_cache.shape[1]
    columns = w_query.shape[1]
    kv_local = key_cache.shape[2] // HEAD
    group = columns // (kv_local * HEAD)
    cw = chunk_width(hidden, n_kv)
    vmem = pl.BlockSpec(memory_space=pltpu.VMEM)
    hbm = pl.BlockSpec(memory_space=pl.ANY)
    ffn_buffers = [
        pltpu.VMEM((n_kv, batch, 2 * cw + LANES), BF16),
        pltpu.VMEM((n_kv - 1, batch, 2 * cw + LANES), BF16),
        pltpu.VMEM((batch, cw), BF16),
        pltpu.VMEM((batch, n_kv * cw), BF16),
    ]
    tp_buffers = [pltpu.VMEM((batch, depth), BF16), pltpu.VMEM((n_tp - 1, batch, depth), BF16)]

    def params(number):
        return pltpu.CompilerParams(
            collective_id=number, has_side_effects=True, vmem_limit_bytes=VMEM_LIMIT
        )

    h1, queries = pl.pallas_call(
        functools.partial(first_kernel, n_kv, n_tp),
        out_shape=(
            jax.ShapeDtypeStruct((batch, depth), F32),
            jax.ShapeDtypeStruct((batch, columns), BF16),
        ),
        in_specs=[vmem] * 3 + [hbm] * 4,
        out_specs=(vmem, vmem),
        scratch_shapes=[
            pltpu.VMEM(first_gate.shape, BF16),
            pltpu.VMEM(first_up.shape, BF16),
            pltpu.VMEM(first_down.shape, BF16),
            pltpu.VMEM(w_query.shape, BF16),
            pltpu.VMEM((n_tp,) + tokens.shape, BF16),
            *ffn_buffers,
            *tp_buffers,
            pltpu.VMEM((batch, columns + LANES), BF16),
            pltpu.VMEM((n_kv - 1, batch, columns + LANES), BF16),
            pltpu.SemaphoreType.DMA((4,)),
            dma_sems(n_tp),
            dma_sems(n_kv),
            dma_sems(n_kv),
            dma_sems(n_tp),
            dma_sems(n_kv),
        ],
        compiler_params=params(1),
    )(
        tokens, first_gain.reshape(1, -1), mix_gain.reshape(1, -1),
        first_gate, first_up, first_down, w_query,
    )

    per_tile = TILE // (MAPS * group)
    q = queries.reshape(batch, kv_local, 1, group, HEAD)
    half = (jnp.arange(HEAD) // (HEAD // MAPS))[None, :] == jnp.arange(MAPS)[:, None]
    q = jnp.where(half[None, None, :, None, :], q, 0).reshape(batch, kv_local, 1, MAPS * group, 1, HEAD)
    place = (jnp.arange(batch) % per_tile)[:, None] == jnp.arange(per_tile)[None, :]
    own = jnp.arange(kv_local)[:, None] == jnp.arange(kv_local)[None, :]
    keep = place[:, None, :, None, None, None] & own[None, :, None, None, :, None]
    q = jnp.where(keep, q, 0).reshape(batch, kv_local * TILE, kv_local * HEAD)

    each = batch // n_kv
    slab_rows = each // per_tile * TILE
    o_part, lse_part = pl.pallas_call(
        functools.partial(attention_kernel, kv_local, per_tile, 1.0 / math.sqrt(HEAD // MAPS)),
        grid=(n_kv,),
        out_shape=(
            jax.ShapeDtypeStruct((n_kv, slab_rows, kv_local * HEAD), BF16),
            jax.ShapeDtypeStruct((n_kv, slab_rows, LANES), F32),
        ),
        in_specs=[
            pl.BlockSpec((each, kv_local * TILE, kv_local * HEAD), lambda i: (i, 0, 0)),
            pl.BlockSpec((each, length, kv_local * HEAD), lambda i: (i, 0, 0)),
            pl.BlockSpec((each, length, kv_local * HEAD), lambda i: (i, 0, 0)),
        ],
        out_specs=(
            pl.BlockSpec((1, slab_rows, kv_local * HEAD), lambda i: (i, 0, 0)),
            pl.BlockSpec((1, slab_rows, LANES), lambda i: (i, 0, 0)),
        ),
        compiler_params=pltpu.CompilerParams(vmem_limit_bytes=VMEM_LIMIT),
    )(q, key_cache, value_cache)

    weight = jnp.repeat(map_weight.reshape(kv_local, group).T, HEAD, axis=1)
    weight = jnp.tile(weight, (slab_rows // group, 1))
    gain = jnp.tile(head_gain, kv_local).reshape(1, -1)
    width = depth // n_tp
    return pl.pallas_call(
        functools.partial(second_kernel, n_kv, n_tp, kv_local, group),
        out_shape=jax.ShapeDtypeStruct((batch, width), BF16),
        in_specs=[vmem] * 6 + [hbm] * 4,
        out_specs=vmem,
        scratch_shapes=[
            pltpu.VMEM(w_out.shape, BF16),
            pltpu.VMEM(second_gate.shape, BF16),
            pltpu.VMEM(second_up.shape, BF16),
            pltpu.VMEM(second_down.shape, BF16),
            pltpu.VMEM((n_kv - 1,) + o_part.shape[1:], BF16),
            pltpu.VMEM((n_kv - 1,) + lse_part.shape[1:], F32),
            pltpu.VMEM(o_part.shape[1:], BF16),
            pltpu.VMEM(o_part.shape, BF16),
            *ffn_buffers,
            *tp_buffers,
            pltpu.VMEM((n_tp, batch, width), BF16),
            pltpu.VMEM((n_tp - 1, batch, width), BF16),
            pltpu.SemaphoreType.DMA((4,)),
            dma_sems(n_kv),
            dma_sems(n_kv),
            dma_sems(n_kv),
            dma_sems(n_kv),
            dma_sems(n_kv),
            dma_sems(n_tp),
            dma_sems(n_tp),
        ],
        compiler_params=params(2),
    )(
        h1, o_part, lse_part, weight, gain, second_gain.reshape(1, -1),
        w_out, second_gate, second_up, second_down,
    )


def solution(mesh):
    placed = (
        P(None, ("kv", "tp")),
        P("kv"),
        P("kv", "tp"),
        P("kv", "tp"),
        P("tp", "kv"),
        P("kv"),
        P("kv", "tp"),
        P(None, "kv", "tp"),
        P(None, "kv", "tp"),
        P("tp"),
        P(),
        P("tp", "kv"),
        P("kv"),
        P("kv", "tp"),
        P("kv", "tp"),
        P("tp", "kv"),
    )
    return jax.shard_map(
        functools.partial(on_device, mesh.shape["kv"], mesh.shape["tp"]),
        mesh=mesh,
        in_specs=placed,
        out_specs=P(None, ("kv", "tp")),
        check_vma=False,
    )
```

time: 629 us -> 111 us (0.18)
  blocking collectives: 259 us -> 0 us
  waiting for transfers between devices: 236 us -> 0 us
  Pallas kernels: 0 us -> 104 us
  local copies, waits for them, and re-layouts: 58.6 us -> 5.33 us
  matrix products: 44.7 us -> 0 us
  between operations: 13.7 us -> 0.09 us
  other arithmetic: 14.3 us -> 0.99 us
    psum x6 -> x0, waiting for transfers between devices: 236 us -> none  [the longest x2 107 us: channel_mixer(): gate_sum, up_sum = lax.psum((part_gate, part_up), 'kv')]
    all_gather x7 -> x0, blocking collectives: 195 us -> none  [the longest x6 189 us: merged(): pieces = jax.tree.map(lambda part: lax.all_gather(part, axis), value)]
    pallas_call x0 -> x3, Pallas kernels: none -> 104 us  [the longest x1 44.6 us: on_device(): pl.pallas_call(functools.partial(second_kernel, n_kv, n_tp, kv_local, gro...]
    psum x3 -> x0, blocking collectives: 63.8 us -> none  [norm_total(): return lax.psum(squares, 'kv')]
    dot_general x12 -> x0, matrix products: 44.7 us -> none  [the longest x2 16.9 us: partial_map(): jnp.einsum('bkgp,bpkd->bkgd', exp_terms.astype(jnp.bfloat16), stored, pre...]
    unnamed x36 -> x5, local copies, waits for them, and re-layouts: 45.2 us -> 1.3 us
    add x21 -> x0, other arithmetic: 7.29 us -> none  [the longest x7 6.86 us: merge_pair(): first[2] * scale_first[..., None] + second[2] * scale_second[..., None]]
  transfers between devices with their start and end apart: 6 -> 0, of which waited for: 5 -> 0; matrix products, arithmetic and copies ran while one was open for 7% -> 0% of each run, Pallas kernels for 0% -> 0%
where the time goes in v1:
time: 111 us
  Pallas kernels  104 us (94%)
  local copies, waits for them, and re-layouts  5.33 us (5%)
    pallas_call x1, Pallas kernels, on_device(): pl.pallas_call(functools.partial(second_kernel, n_kv, n_tp, kv_local, gro...  44.6 us
    pallas_call x1, Pallas kernels, on_device(): pl.pallas_call(functools.partial(first_kernel, n_kv, n_tp), out_shape=(ja...  40.9 us
    pallas_call x1, Pallas kernels, on_device(): pl.pallas_call(functools.partial(attention_kernel, kv_local, per_tile, 1....  18.8 us

profile of v1, /device:TPU:0, one launch (start us, length us, event | category | flops | bytes accessed | tf_op | source)
XLA Modules:
  0.0 110.8 jit_solution(15031295447699216624)
XLA Ops:
  0.0 40.9 %shard_map.154 = (f32[32,512]{1,0:T(8,128)}, bf16[32,512]{1,0:T(8,128)(2,1)}) custom-call(bf16[32,128]{1,0:T(8,128)(2,1)} %tokens.1, f32[1,512]{1,0:T(1,128)} %bitcast.7, f32[1,512]{1,0:T(1,128)} %bitcast.8, bf16[512,2816]{1,0:T(8,128)(2,1)} %gate_any.2, bf16[512,2816]{1,0:T(8,128)(2,1)} %up_any.2, bf16[2816,512]{1,0:T(8,128)(2,1)} %down_any.2, ...), custom_call_target="tpu_custom_call" | custom-call | tf_op jit(solution)/shard_map/pallas_call | solution.py:298
  41.0 0.1 iota_compare_fusion
  41.0 0.1 broadcast_and_fusion
  41.2 0.9 broadcast_in_dim.64
  42.1 0.1 broadcast_in_dim.65
  42.2 0.1 broadcast_select_fusion.1
  42.3 0.7 broadcast_select_fusion
  43.0 1.5 %select_n.40.q_ref = bf16[32,32,256]{2,1,0:T(8,128)(2,1)} reshape(bf16[32,4,2,4,4,64]{5,4,3,2,1,0:T(4,128)(2,1)S(1)} %broadcast_select_fusion) | data formatting | bytes 1048576 | tf_op jit(solution)/shard_map/jit(_where)/select_n | solution.py:336
  44.4 0.0 copy-start
  44.4 0.0 copy-start.1
  44.4 18.8 %shard_map.155 = (bf16[8,16,256]{2,1,0:T(8,128)(2,1)}, f32[8,16,128]{2,1,0:T(8,128)}) custom-call(bf16[32,32,256]{2,1,0:T(8,128)(2,1)} %select_n.40.q_ref, bf16[32,1024,256]{2,1,0:T(8,128)(2,1)} %k_ref.1, bf16[32,1024,256]{2,1,0:T(8,128)(2,1)} %v_ref.1), custom_call_target="tpu_custom_call" | custom-call | tf_op jit(solution)/shard_map/pallas_call | solution.py:340
  63.3 0.0 copy-done
  63.3 0.1 reshape.116
  63.4 0.1 copy.18
  63.5 0.1 broadcast_in_dim.70
  63.5 0.1 tile.16
  63.6 0.6 tile.18.map_weight
  64.2 0.0 copy-done.1
  64.3 0.6 reshape_tile.3.head_gain
  64.9 44.6 %shard_map.156 = bf16[32,128]{1,0:T(8,128)(2,1)} custom-call(f32[32,512]{1,0:T(8,128)} %get-tuple-element.9.h_in, bf16[8,16,256]{2,1,0:T(8,128)(2,1)} %get-tuple-element.11.o_part, f32[8,16,128]{2,1,0:T(8,128)} %get-tuple-element.12.lse_part, f32[16,256]{1,0:T(8,128)} %tile.18.map_weight, f32[1,256]{1,0:T(1,128)} %reshape_tile.3.head_gain, ...), custom_call_target="tpu_custom_call" | custom-call | tf_op jit(solution)/shard_map/pallas_call | solution.py:363
  109.5 1.3 %copy.20 = bf16[32,128]{1,0:T(8,128)(2,1)} copy(bf16[32,128]{1,0:T(8,128)(2,1)} %shard_map.156) | data formatting | bytes 16384
  (8 shorter events, 0.1 us)
Async XLA Ops:
  44.4 18.9 %copy-start = (f32[8]{0:T(128)S(1)}, f32[8]{0:T(128)}, u32[]{:S(2)}) copy-start(f32[8]{0:T(128)} %param.25) | copy-start | bytes 100
  44.4 19.8 %copy-start.1 = (f32[64]{0:T(128)S(1)}, f32[64]{0:T(128)}, u32[]{:S(2)}) copy-start(f32[64]{0:T(128)} %param.26) | copy-start | bytes 772
